TPU v7x, 32 devices: a whole 2x2x4 slice. The times are simulated.
32 devices in a mesh: vp: 4 (over y, x), dp: 8 (over z, core).
Axes of the slice: x: 2, y: 2, z: 4, core: 2. Of those that a mesh axis runs over, the one named last changes fastest.
Arguments:
- hidden_act: bfloat16 [4096, 8192], P('dp', 'vp'), may hold values from 0 to 36
- down_weight: bfloat16 [8192, 2048], P('vp'), may hold values from -0.0625 to 0.0625
- residual: bfloat16 [4096, 2048], P(('dp', 'vp')), may hold values from -300 to 300
- post_gain: float32 [2048], replicated, may hold values from 0.1 to 1.9
- final_gain: float32 [2048], replicated, may hold values from 0.1 to 1.9
- vocab: bfloat16 [2048, 32768], P(None, 'vp'), may hold values from -0.33 to 0.33
- vocab_bias: float32 [32768], P('vp'), may hold values from -2.5 to 2.5
- target_ids: int32 [4096, 4], P('dp'), may hold values from 0 to 32767
- target_weights: float32 [4096, 4], P('dp'), may hold values from 0 to 1, as said below
Outputs:
- losses: float32 [4096], P(('dp', 'vp'))
- stream_grad: float32 [4096, 2048], P(('dp', 'vp'))
- vocab_grad: float32 [2048, 32768], P('dp', 'vp')
Inputs may be any that keep to these rules, and one draw needn't show every extreme that they name: `target_weights`: the 4 weights of a token add up to one.
All inputs are finite; a program needn't handle non-finite values.
Results may differ from a plain program's by a relative error of at most 0.01225.
Values may be sent and summed in bfloat16 or wider, within the bound.
A program may use at most 192 MiB of HBM per device.

v0:
```python
import jax
import jax.numpy as jnp
from jax import lax
from jax.sharding import PartitionSpec as P

CHUNKS = 4


epsilon = 1e-06
z_weight = 0.001
loss_scale = 32.0


def inverse_rms(values):
    return lax.rsqrt(jnp.mean(values * values, axis=-1, keepdims=True) + epsilon)


def shards(
    hidden_act,
    down_weight,
    residual,
    post_gain,
    final_gain,
    vocab,
    vocab_bias,
    target_ids,
    target_weights,
):
    own_rows = residual.shape[0]
    group_rows = hidden_act.shape[0]
    columns = vocab.shape[1]
    vp_index = lax.axis_index("vp")
    branch = lax.psum_scatter(
        jnp.dot(hidden_act, down_weight, preferred_element_type=jnp.float32),
        "vp",
        scatter_dimension=0,
        tiled=True,
    )
    stream = residual.astype(jnp.float32) + branch * inverse_rms(branch) * post_gain
    inverse = inverse_rms(stream)
    normed = (stream * inverse * final_gain).astype(jnp.bfloat16)
    gathered = lax.all_gather(normed, "vp", axis=0, tiled=True)
    local_ids = target_ids - vp_index * columns
    position = lax.broadcasted_iota(jnp.int32, (1, columns), 1)
    wanted = jnp.zeros((group_rows, columns), jnp.float32)
    for target_k in range(target_ids.shape[1]):
        wanted = wanted + jnp.where(
            local_ids[:, target_k : target_k + 1] == position,
            target_weights[:, target_k : target_k + 1],
            0.0,
        )
    scores = jnp.dot(gathered, vocab, preferred_element_type=jnp.float32) + vocab_bias[None, :]
    local_max = jnp.max(scores, axis=1)
    local_sum = jnp.sum(jnp.exp(scores - local_max[:, None]), axis=1)
    local_target = jnp.sum(wanted * scores, axis=1)
    stats = lax.all_gather(jnp.stack([local_max, local_sum, local_target]), "vp", axis=0)
    row_max = jnp.max(stats[:, 0], axis=0)
    row_sum = jnp.sum(stats[:, 1] * jnp.exp(stats[:, 0] - row_max), axis=0)
    target_score = jnp.sum(stats[:, 2], axis=0)
    log_norm = row_max + jnp.log(row_sum)
    group_losses = log_norm - target_score + z_weight * log_norm * log_norm
    losses = lax.dynamic_slice_in_dim(group_losses, vp_index * own_rows, own_rows, 0)
    factor = (1.0 + 2.0 * z_weight * log_norm)[:, None]
    probability = jnp.exp(scores - log_norm[:, None])
    score_grads = (loss_scale * (probability * factor - wanted)).astype(jnp.bfloat16)
    chunk = columns // CHUNKS
    pieces = []
    for index in range(CHUNKS):
        part = score_grads[:, index * chunk : (index + 1) * chunk]
        grad = lax.dot_general(
            gathered, part, (((0,), (0,)), ((), ())), preferred_element_type=jnp.float32
        ).astype(jnp.bfloat16)
        pieces.append(lax.psum_scatter(grad, "dp", scatter_dimension=0, tiled=True))
    row_grad = lax.psum_scatter(
        lax.dot_general(
            score_grads, vocab, (((1,), (1,)), ((), ())), preferred_element_type=jnp.float32
        ),
        "vp",
        scatter_dimension=0,
        tiled=True,
    )
    vocab_grad = jnp.concatenate([piece.astype(jnp.float32) for piece in pieces], axis=1)
    upstream = row_grad * final_gain
    stream_grad = inverse * (
        upstream - stream * inverse * inverse * jnp.mean(upstream * stream, axis=-1, keepdims=True)
    )
    return (losses, stream_grad, vocab_grad)


def solution(mesh):
    in_specs = (
        P("dp", "vp"),
        P("vp", None),
        P(("dp", "vp"), None),
        P(),
        P(),
        P(None, "vp"),
        P("vp"),
        P("dp", None),
        P("dp", None),
    )
    out_specs = (P(("dp", "vp")), P(("dp", "vp"), None), P("dp", "vp"))
    return jax.shard_map(shards, mesh=mesh, in_specs=in_specs, out_specs=out_specs, check_vma=False)
```

profile of v0, /device:TPU:8, one launch (start us, length us, event | category | flops | bytes accessed | tf_op | source)
XLA Modules:
  0.0 633.1 jit_solution(9418689511885468283)
XLA Ops:
  7.2 0.0 copy-start
  7.2 0.0 copy-start.6
  7.2 0.0 copy-start.4
  7.2 0.0 copy-start.7
  7.2 0.0 reduce-scatter.7.cloned.1.call-start
  7.3 1.5 copy-done
  8.8 9.4 %fusion.12 = f32[512,2048]{1,0:T(8,128)} fusion(bf16[512,2048]{1,0:T(8,128)(2,1)S(1)} %copy-done, bf16[2048,2048]{1,0:T(8,128)(2,1)} %param.10), kind=kOutput, calls=%fused_computation.43 | convolution fusion | flops 4294967296 | bytes 14680064 | tf_op jit(solution)/shard_map/dot_general | solution.py:34
  18.1 0.0 reduce-scatter.7.cloned.1.call-update
  18.2 0.0 all-gather.4.cloned.1.call-start
  18.2 53.9 %reduce-scatter.7.cloned.1.call-done = f32[128,2048]{1,0:T(8,128)} async-done(((f32[512,2048]{1,0:T(8,128)}), f32[128,2048]{1,0:T(8,128)}) %reduce-scatter.7.cloned.1.call-update) | async-done | bytes 1048592 | tf_op jit(solution)/shard_map/reduce_scatter | solution.py:33
  72.1 1.4 multiply_reduce_fusion.3
  73.5 1.6 multiply_reduce_fusion.2
  75.1 0.0 copy-done.7
  75.1 2.3 multiply_convert_fusion.1
  77.4 0.0 all-gather.4.cloned.1.call-update
  77.4 0.6 reduce-scatter.9.cloned.1.call-start
  78.0 0.0 copy-done.8
  78.0 0.0 copy-done.9
  78.1 34.7 %all-gather.4.cloned.1.call-done = bf16[512,2048]{1,0:T(8,128)(2,1)} async-done(((bf16[128,2048]{1,0:T(8,128)(2,1)}), bf16[512,2048]{1,0:T(8,128)(2,1)}) %all-gather.4.cloned.1.call-update) | async-done | bytes 2097168 | tf_op jit(solution)/shard_map/all_gather | solution.py:42
  112.7 27.3 %add_reduce_fusion = (f32[512]{0:T(512)S(1)}, f32[512,8192]{1,0:T(8,128)}) fusion(f32[8192]{0:T(1024)S(1)} %copy-done.5, bf16[512,2048]{1,0:T(8,128)(2,1)} %all-gather.4.cloned.1.call-done, bf16[2048,8192]{1,0:T(8,128)(2,1)} %param.14), kind=kOutput, calls=%fused_computation.8 | convolution fusion | flops 17188257792 | bytes 52463616 | tf_op jit(solution)/shard_map/dot_general | solution.py:52
  140.0 16.2 %exponential_reduce_fusion = (f32[512]{0:T(512)S(1)}, f32[512]{0:T(512)S(1)}) fusion(f32[512,8192]{1,0:T(8,128)} %get-tuple-element.22, f32[512]{0:T(512)S(1)} %get-tuple-element.21, f32[8192]{0:T(1024)S(1)} %copy-done.5, f32[512]{0:T(512)S(1)} %bitcast.39, s32[512]{0:T(512)S(1)} %bitcast.45, f32[512]{0:T(512)S(1)} %bitcast.41, s32[512]{0:T(512)S(1)} %bitcast.47, ...), kind=kLoop, calls=%fused_computation.7 | loop fusion | flops 67107840 | bytes 16832512 | tf_op jit(solution)/shard_map/reduce_sum | solution.py:54
  156.3 8.3 %all-gather.1 = f32[4,3,512]{2,1,0:T(4,128)S(1)} all-gather(f32[1,3,512]{2,1,0:T(4,128)S(1)} %maximum_bitcast_fusion), channel_id=2, replica_groups=mesh['vp'=4,'dp'=8] {'vp'}, dimensions={0}, use_global_device_ids=true | all-gather | bytes 30720 | tf_op jit(solution)/shard_map/all_gather | solution.py:56
  164.7 0.0 copy-done.2
  164.7 18.7 %multiply_convert_fusion = bf16[512,8192]{1,0:T(8,128)(2,1)} fusion(f32[512,8192]{1,0:T(8,128)S(1)} %copy-done.2, f32[512]{0:T(512)S(1)} %get-tuple-element.7, f32[512]{0:T(512)S(1)} %get-tuple-element.8, f32[512]{0:T(512)S(1)} %bitcast.40, s32[512]{0:T(512)S(1)} %bitcast.46, f32[512]{0:T(512)S(1)} %bitcast.42, s32[512]{0:T(512)S(1)} %bitcast.48, ...), kind=kLoop, calls=%fused_computation | loop fusion | flops 71303168 | bytes 25219072 | tf_op jit(solution)/shard_map/convert_element_type | solution.py:65
  183.4 24.9 %fusion.13 = f32[512,2048]{1,0:T(8,128)} fusion(bf16[512,8192]{1,0:T(8,128)(2,1)} %multiply_convert_fusion, bf16[2048,8192]{1,0:T(8,128)(2,1)} %param.14), kind=kOutput, calls=%fused_computation.44 | convolution fusion | flops 17179869184 | bytes 46137344 | tf_op jit(solution)/shard_map/dot_general | solution.py:75
  208.3 0.0 reduce-scatter.9.cloned.1.call-update
  208.3 0.3 reduce-scatter.17.cloned.1.call-start
  208.6 10.0 %convolution_convert_fusion = bf16[2048,2048]{1,0:T(8,128)(2,1)} fusion(bf16[512,2048]{1,0:T(8,128)(2,1)} %all-gather.4.cloned.1.call-done, bf16[512,8192]{1,0:T(8,128)(2,1)} %multiply_convert_fusion), kind=kOutput, calls=%fused_computation.9 | convolution fusion | flops 4299161600 | bytes 12582912 | tf_op jit(solution)/shard_map/dot_general | solution.py:70
  218.6 0.0 reduce-scatter.17.cloned.1.call-update
  218.6 0.0 reduce-scatter.15.cloned.1.call-start
  218.7 10.0 %convolution_convert_fusion.1 = bf16[2048,2048]{1,0:T(8,128)(2,1)} fusion(bf16[512,2048]{1,0:T(8,128)(2,1)} %all-gather.4.cloned.1.call-done, bf16[512,8192]{1,0:T(8,128)(2,1)} %multiply_convert_fusion), kind=kOutput, calls=%fused_computation.10 | convolution fusion | flops 4299161600 | bytes 12582912 | tf_op jit(solution)/shard_map/dot_general | solution.py:70
  228.7 0.0 reduce-scatter.15.cloned.1.call-update
  228.7 0.3 reduce-scatter.13.cloned.1.call-start
  229.0 10.3 %convolution_convert_fusion.2 = bf16[2048,2048]{1,0:T(8,128)(2,1)} fusion(bf16[512,2048]{1,0:T(8,128)(2,1)} %all-gather.4.cloned.1.call-done, bf16[512,8192]{1,0:T(8,128)(2,1)} %multiply_convert_fusion), kind=kOutput, calls=%fused_computation.11 | convolution fusion | flops 4299161600 | bytes 12582912 | tf_op jit(solution)/shard_map/dot_general | solution.py:70
  239.3 0.0 reduce-scatter.13.cloned.1.call-update
  239.3 0.0 reduce-scatter.11.cloned.1.call-start
  239.3 10.1 %convolution_convert_fusion.3 = bf16[2048,2048]{1,0:T(8,128)(2,1)} fusion(bf16[512,2048]{1,0:T(8,128)(2,1)} %all-gather.4.cloned.1.call-done, bf16[512,8192]{1,0:T(8,128)(2,1)} %multiply_convert_fusion), kind=kOutput, calls=%fused_computation.12 | convolution fusion | flops 4299161600 | bytes 12582912 | tf_op jit(solution)/shard_map/dot_general | solution.py:70
  249.4 0.0 reduce-scatter.11.cloned.1.call-update
  249.5 0.6 dynamic_slice.3
  250.1 11.0 %reduce-scatter.9.cloned.1.call-done = f32[128,2048]{1,0:T(8,128)} async-done(((f32[512,2048]{1,0:T(8,128)}), f32[128,2048]{1,0:T(8,128)}) %reduce-scatter.9.cloned.1.call-update) | async-done | bytes 1048592 | tf_op jit(solution)/shard_map/reduce_scatter | solution.py:74
  261.0 1.9 multiply_reduce_fusion.1
  262.9 2.8 subtract_multiply_fusion
  265.7 84.2 %reduce-scatter.17.cloned.1.call-done = bf16[256,2048]{1,0:T(8,128)(2,1)} async-done(((bf16[2048,2048]{1,0:T(8,128)(2,1)}), bf16[256,2048]{1,0:T(8,128)(2,1)}) %reduce-scatter.17.cloned.1.call-update) | async-done | bytes 1048592 | tf_op jit(solution)/shard_map/reduce_scatter | solution.py:73
  350.0 90.2 %reduce-scatter.15.cloned.1.call-done = bf16[256,2048]{1,0:T(8,128)(2,1)} async-done(((bf16[2048,2048]{1,0:T(8,128)(2,1)}), bf16[256,2048]{1,0:T(8,128)(2,1)}) %reduce-scatter.15.cloned.1.call-update) | async-done | bytes 1048592 | tf_op jit(solution)/shard_map/reduce_scatter | solution.py:73
  440.1 90.2 %reduce-scatter.13.cloned.1.call-done = bf16[256,2048]{1,0:T(8,128)(2,1)} async-done(((bf16[2048,2048]{1,0:T(8,128)(2,1)}), bf16[256,2048]{1,0:T(8,128)(2,1)}) %reduce-scatter.13.cloned.1.call-update) | async-done | bytes 1048592 | tf_op jit(solution)/shard_map/reduce_scatter | solution.py:73
  530.3 90.3 %reduce-scatter.11.cloned.1.call-done = bf16[256,2048]{1,0:T(8,128)(2,1)} async-done(((bf16[2048,2048]{1,0:T(8,128)(2,1)}), bf16[256,2048]{1,0:T(8,128)(2,1)}) %reduce-scatter.11.cloned.1.call-update) | async-done | bytes 1048592 | tf_op jit(solution)/shard_map/reduce_scatter | solution.py:73
  620.6 5.3 maximum_convert_fusion
  625.9 0.0 copy-done.1
  (21 shorter events, 0.2 us)
Async XLA Ops:
  7.2 1.6 copy-start
  7.2 66.3 %copy-start.6 = (f32[2048]{0:T(1024)S(1)}, f32[2048]{0:T(1024)}, u32[]{:S(2)}) copy-start(f32[2048]{0:T(1024)} %param.12) | copy-start | bytes 24580
  7.2 66.3 %copy-start.4 = (bf16[128,2048]{1,0:T(8,128)(2,1)S(1)}, bf16[128,2048]{1,0:T(8,128)(2,1)}, u32[]{:S(2)}) copy-start(bf16[128,2048]{1,0:T(8,128)(2,1)} %param.11) | copy-start | bytes 1572868
  7.2 67.9 %copy-start.7 = (f32[2048]{0:T(1024)S(1)}, f32[2048]{0:T(1024)}, u32[]{:S(2)}) copy-start(f32[2048]{0:T(1024)} %param.13) | copy-start | bytes 24580
  7.2 64.9 %reduce-scatter.7.cloned.1.call-start = ((), (), s32[]{:S(2)}) async-start(), calls=%async_computation.6 | async-start | bytes 5242880 | tf_op jit(solution)/shard_map/reduce_scatter | solution.py:33
  18.1 59.9 %copy-start.8 = (f32[512,4]{0,1:T(4,128)S(1)}, f32[512,4]{0,1:T(4,128)}, u32[]{:S(2)}) copy-start(f32[512,4]{0,1:T(4,128)} %param.17) | copy-start | bytes 24580
  18.1 59.9 %copy-start.9 = (s32[512,4]{0,1:T(4,128)S(1)}, s32[512,4]{0,1:T(4,128)}, u32[]{:S(2)}) copy-start(s32[512,4]{0,1:T(4,128)} %param.16) | copy-start | bytes 24580
  18.1 94.6 %copy-start.5 = (f32[8192]{0:T(1024)S(1)}, f32[8192]{0:T(1024)}, u32[]{:S(2)}) copy-start(f32[8192]{0:T(1024)} %param.15) | copy-start | bytes 98308
  18.2 94.6 %all-gather.4.cloned.1.call-start = ((), (), s32[]{:S(2)}) async-start(), calls=%async_computation.7 | async-start | bytes 2621440 | tf_op jit(solution)/shard_map/all_gather | solution.py:42
  77.4 183.6 %reduce-scatter.9.cloned.1.call-start = ((), (), s32[]{:S(2)}) async-start(), calls=%async_computation.8 | async-start | bytes 5242880 | tf_op jit(solution)/shard_map/reduce_scatter | solution.py:74
  140.0 24.6 %copy-start.2 = (f32[512,8192]{1,0:T(8,128)S(1)}, f32[512,8192]{1,0:T(8,128)}, u32[]{:S(2)}) copy-start(f32[512,8192]{1,0:T(8,128)} %get-tuple-element.22) | copy-start | bytes 50331652
  208.3 141.6 %reduce-scatter.17.cloned.1.call-start = ((), (), s32[]{:S(2)}) async-start(), calls=%async_computation.12 | async-start | bytes 9437184 | tf_op jit(solution)/shard_map/reduce_scatter | solution.py:73
  218.6 221.5 %reduce-scatter.15.cloned.1.call-start = ((), (), s32[]{:S(2)}) async-start(), calls=%async_computation.11 | async-start | bytes 9437184 | tf_op jit(solution)/shard_map/reduce_scatter | solution.py:73
  228.7 301.6 %reduce-scatter.13.cloned.1.call-start = ((), (), s32[]{:S(2)}) async-start(), calls=%async_computation.10 | async-start | bytes 9437184 | tf_op jit(solution)/shard_map/reduce_scatter | solution.py:73
  239.3 381.3 %reduce-scatter.11.cloned.1.call-start = ((), (), s32[]{:S(2)}) async-start(), calls=%async_computation.9 | async-start | bytes 9437184 | tf_op jit(solution)/shard_map/reduce_scatter | solution.py:73
  249.4 11.6 %copy-start.3 = (f32[128,2048]{1,0:T(8,128)S(1)}, f32[128,2048]{1,0:T(8,128)}, u32[]{:S(2)}) copy-start(f32[128,2048]{1,0:T(8,128)} %reduce-scatter.7.cloned.1.call-done) | copy-start | bytes 3145732
  261.0 364.9 %copy-start.1 = (bf16[512,2048]{1,0:T(8,128)(2,1)S(1)}, bf16[512,2048]{1,0:T(8,128)(2,1)}, u32[]{:S(2)}) copy-start(bf16[512,2048]{1,0:T(8,128)(2,1)} %param.9) | copy-start | bytes 6291460
Sparse Core Ops, SparseCore 0:
  18.3 53.7 reduce-scatter.6
  77.5 35.1 all-gather.3
  208.4 52.5 reduce-scatter.8
  263.2 86.7 reduce-scatter.16
  352.1 87.9 reduce-scatter.14
  442.3 87.9 reduce-scatter.12
  532.6 87.9 reduce-scatter.10
where the time goes:
time: 640 us; the launch traced here: 633 us
  waiting for transfers between devices  455 us (71%)
  matrix products  102 us (16%)
  other arithmetic  50.3 us (8%)
  between operations  14.5 us (2%)
  blocking collectives  8.32 us (1%)
    reduce_scatter x4, waiting for transfers between devices, shards(): pieces.append(lax.psum_scatter(grad, 'dp', scatter_dimension=0, tiled=True))  355 us
    reduce_scatter x1, waiting for transfers between devices, shards(): lax.psum_scatter(jnp.dot(hidden_act, down_weight, preferred_element_type=...  53.9 us
    dot_general x4, matrix products, shards(): lax.dot_general(gathered, part, (((0,), (0,)), ((), ())), preferred_eleme...  40.4 us
    all_gather x1, waiting for transfers between devices, shards(): gathered = lax.all_gather(normed, 'vp', axis=0, tiled=True)  34.7 us
    dot_general x1, matrix products, shards(): jnp.dot(gathered, vocab, preferred_element_type=jnp.float32)  27.3 us
    dot_general x1, matrix products, shards(): lax.dot_general(score_grads, vocab, (((1,), (1,)), ((), ())), preferred_e...  24.9 us
    convert_element_type x1, other arithmetic, shards(): (loss_scale * (probability * factor - wanted)).astype(jnp.bfloat16)  18.7 us
    reduce_sum x1, other arithmetic, shards(): local_sum = jnp.sum(jnp.exp(scores - local_max[:, None]), axis=1)  16.2 us
  transfers between devices with their start and end apart: 7, of which 7 were waited for; matrix products, arithmetic and copies ran while one was open for 7% of the time, Pallas kernels for 0%

commit v1 on v0

--- a/solution.py
+++ b/solution.py
@@ -1,21 +1,839 @@
+import functools
+
 import jax
 import jax.numpy as jnp
 from jax import lax
+from jax.experimental import pallas as pl
+from jax.experimental.pallas import tpu as pltpu
 from jax.sharding import PartitionSpec as P
 
+MESH = pl.DeviceIdType.MESH
+CORES = 2
+PLANE = 4
+TILE = 512
 CHUNKS = 4
-
 
 epsilon = 1e-06
 z_weight = 0.001
 loss_scale = 32.0
+f32 = jnp.float32
+bf16 = jnp.bfloat16
+
+
+def remote(src, dst, send_sem, recv_sem, vp, dp):
+    return pltpu.make_async_remote_copy(
+        src_ref=src,
+        dst_ref=dst,
+        send_sem=send_sem,
+        recv_sem=recv_sem,
+        device_id={"vp": vp, "dp": dp},
+        device_id_type=MESH,
+    )
+
+
+class Place:
+    def __init__(self, nz):
+        self.nz = nz
+        self.p = lax.axis_index("vp")
+        self.dp = lax.axis_index("dp")
+        self.z = self.dp // CORES
+        self.c = lax.rem(self.dp, CORES)
+        self.px = self.p + 1 - 2 * lax.rem(self.p, 2)
+        self.py = lax.rem(self.p + 2, PLANE)
+        self.pd = PLANE - 1 - self.p
+        self.plane = (self.px, self.py, self.pd)
+
+    def at(self, z):
+        return z * CORES + self.c
+
+    def ahead(self, k):
+        return lax.rem(self.z + k, self.nz)
+
+    def behind(self, k):
+        return lax.rem(self.z - k + self.nz, self.nz)
+
+
+def greet(peers):
+    barrier = pltpu.get_barrier_semaphore()
+    for vp, dp in peers:
+        pl.semaphore_signal(barrier, inc=1, device_id={"vp": vp, "dp": dp}, device_id_type=MESH)
+    pl.semaphore_wait(barrier, len(peers))
+
+
+def rows_to_column(row):
+    n = row.shape[1]
+    eye = lax.broadcasted_iota(jnp.int32, (n, n), 0) == lax.broadcasted_iota(jnp.int32, (n, n), 1)
+    return jnp.sum(jnp.where(eye, row, 0.0), axis=1, keepdims=True)
+
+
+def column_to_row(column):
+    n = column.shape[0]
+    eye = lax.broadcasted_iota(jnp.int32, (n, n), 0) == lax.broadcasted_iota(jnp.int32, (n, n), 1)
+    return jnp.sum(jnp.where(eye, column, 0.0), axis=0, keepdims=True)
+
+
+def forward_kernel(
+    nz,
+    topk,
+    hidden,
+    down_hbm,
+    resid,
+    post_gain,
+    final_gain,
+    vocab_hbm,
+    bias,
+    target,
+    normed_hbm,
+    grads_hbm,
+    stream_out,
+    losses_out,
+    down,
+    vocab,
+    partial,
+    own,
+    tosend,
+    arrived,
+    gathered,
+    scores,
+    targets,
+    columns_of,
+    lse_col,
+    tgt_col,
+    stat,
+    stat_plane,
+    stat_mid,
+    stat_line,
+    grads,
+    down_sem,
+    vocab_sem,
+    tgt_send,
+    tgt_recv,
+    rs_send,
+    rs_recv,
+    ag_send,
+    ag_recv,
+    st_send,
+    st_recv,
+    out_sem,
+    grads_sem,
+):
+    me = Place(nz)
+    p, z, c = me.p, me.z, me.c
+    rows, width = resid.shape
+    group = hidden.shape[0]
+    span = vocab.shape[1]
+    tiles = width // TILE
+
+    def down_copy(t):
+        cut = pl.ds(pl.multiple_of(t * TILE, TILE), TILE)
+        return pltpu.make_async_copy(down_hbm.at[:, cut], down.at[:, cut], down_sem.at[t])
+
+    for t in range(tiles):
+        down_copy(t).start()
+    vocab_copy = pltpu.make_async_copy(
+        vocab_hbm.at[:, pl.ds(pl.multiple_of(z * span, span), span)], vocab, vocab_sem
+    )
+    vocab_copy.start()
+
+    line = [(p, me.at(me.ahead(k))) for k in range(1, nz)]
+    greet([(q, me.dp) for q in me.plane] + line)
+
+    def target_copy(k):
+        return remote(target, targets.at[z], tgt_send.at[k - 1], tgt_recv.at[k - 1], p, me.at(me.ahead(k)))
+
+    for k in range(1, nz):
+        target_copy(k).start()
+    targets[z] = target[...]
+
+    def piece(kind, t):
+        q = me.plane[kind]
+        cut = pl.ds(pl.multiple_of(t * TILE, TILE), TILE)
+        return remote(
+            tosend.at[pl.ds(pl.multiple_of(q * rows, rows), rows), cut],
+            arrived.at[kind, :, cut],
+            rs_send.at[kind, t],
+            rs_recv.at[kind, t],
+            q,
+            me.dp,
+        )
+
+    def down_tile(t, _):
+        down_copy(t).wait()
+        cut = pl.ds(pl.multiple_of(t * TILE, TILE), TILE)
+        partial[...] = jnp.dot(hidden[...], down[:, cut], preferred_element_type=f32)
+        tosend[:, cut] = partial[...].astype(bf16)
+        own[:, cut] = partial[pl.ds(pl.multiple_of(p * rows, rows), rows), :]
+        for kind in (2, 0, 1):
+            piece(kind, t).start()
+        return 0
+
+    lax.fori_loop(0, tiles, down_tile, 0)
+    for t in range(tiles):
+        for kind in range(3):
+            piece(kind, t).wait_recv()
+
+    step = 16
+
+    def norm_rows(i, _):
+        r = pl.ds(pl.multiple_of(i * step, step), step)
+        branch = own[r, :]
+        for kind in range(3):
+            branch = branch + arrived[kind, r, :].astype(f32)
+        scale = lax.rsqrt(jnp.mean(branch * branch, axis=1, keepdims=True) + epsilon)
+        stream = resid[r, :].astype(f32) + branch * scale * post_gain[...]
+        inverse = lax.rsqrt(jnp.mean(stream * stream, axis=1, keepdims=True) + epsilon)
+        stream_out[r, :] = stream
+        gathered[z, pl.ds(pl.multiple_of(p * rows + i * step, step), step), :] = (
+            stream * inverse * final_gain[...]
+        ).astype(bf16)
+        return 0
+
+    lax.fori_loop(0, rows // step, norm_rows, 0)
+
+    def block(zz, q):
+        return gathered.at[zz, pl.ds(pl.multiple_of(q * rows, rows), rows), :]
+
+    def send(zz, q, way, kind, vp, dp):
+        return remote(block(zz, q), block(zz, q), ag_send.at[zz, way], ag_recv.at[zz, kind], vp, dp)
+
+    def to_x(zz):
+        return send(zz, p, 0, 1, me.px, me.dp)
+
+    def to_y(zz):
+        return send(zz, p, 1, 2, me.py, me.dp)
+
+    def up(zz):
+        return send(zz, p, 2, 0, p, me.dp + CORES)
+
+    def below(zz):
+        return send(zz, p, 3, 0, p, me.dp - CORES)
+
+    def corner_y(zz):
+        return send(zz, me.px, 4, 3, me.py, me.dp)
+
+    def corner_x(zz):
+        return send(zz, me.py, 4, 3, me.px, me.dp)
+
+    def landed(zz, kind, q):
+        return remote(block(zz, q), block(zz, q), ag_send.at[zz, 0], ag_recv.at[zz, kind], p, me.dp)
+
+    def column_stage(s, zz):
+        @pl.when(s > 0)
+        def _():
+            landed(zz, 0, p).wait_recv()
+
+        @pl.when((zz <= z) & (z + 1 < nz))
+        def _():
+            up(zz).start()
+
+        @pl.when((zz >= z) & (z > 0))
+        def _():
+            below(zz).start()
+
+        to_x(zz).start()
+        to_y(zz).start()
+
+    def corner_stage(zz):
+        landed(zz, 1, me.px).wait_recv()
+
+        @pl.when(lax.rem(zz, 2) == 0)
+        def _():
+            corner_y(zz).start()
+
+        landed(zz, 2, me.py).wait_recv()
+
+        @pl.when(lax.rem(zz, 2) == 1)
+        def _():
+            corner_x(zz).start()
+
+    first_column = p * vocab_hbm.shape[1] + z * span
+    position = lax.broadcasted_iota(jnp.int32, (1, span), 1).astype(f32)
+    chunk = 32
+    lanes = 128
+
+    def wanted_of(zz, r):
+        total = None
+        for k in range(topk):
+            ids = columns_of[zz, r, k : k + 1] - first_column.astype(f32)
+            weight = columns_of[zz, r, topk + k : topk + k + 1]
+            term = jnp.where(ids == position, weight, 0.0)
+            total = term if total is None else total + term
+        return total
+
+    row_at = lax.broadcasted_iota(jnp.int32, (2 * nz, lanes), 0)
+    stat[...] = jnp.zeros_like(stat)
+
+    def row_of(ref, q, cut):
+        return jnp.sum(jnp.where(row_at == q, ref[:, cut], 0.0), axis=0, keepdims=True)
+
+    def compute_stage(zz):
+        landed(zz, 3, me.pd).wait_recv()
+
+        def tile(t, _):
+            cut = pl.ds(pl.multiple_of(t * TILE, TILE), TILE)
+            at = pl.ds(pl.multiple_of(z * span + t * TILE, TILE), TILE)
+            scores[zz, :, cut] = (
+                jnp.dot(gathered[zz], vocab[:, cut], preferred_element_type=f32) + bias[:, at]
+            )
+            return 0
+
+        lax.fori_loop(0, span // TILE, tile, 0)
+
+        def stats(i, _):
+            r = pl.ds(pl.multiple_of(i * chunk, chunk), chunk)
+            values = scores[zz, r, :]
+            largest = jnp.max(values, axis=1, keepdims=True)
+            total = jnp.sum(jnp.exp(values - largest), axis=1, keepdims=True)
+            lse_col[r, :] = largest + jnp.log(total)
+            tgt_col[r, :] = jnp.sum(wanted_of(zz, r) * values, axis=1, keepdims=True)
+            return 0
+
+        lax.fori_loop(0, group // chunk, stats, 0)
+        for j in range(group // lanes):
+            cut = slice(j * lanes, (j + 1) * lanes)
+            kept = jnp.where(row_at == zz, column_to_row(lse_col[cut, :]), stat[:, cut])
+            stat[:, cut] = jnp.where(row_at == nz + zz, column_to_row(tgt_col[cut, :]), kept)
+
+    steps = 2 * nz - 1
+    lag = 2
+
+    def gather_step(i, _):
+        def staged(s, stage):
+            half = (s + 1) // 2
+            zz = z + half * (1 - 2 * lax.rem(s, 2))
+
+            @pl.when((zz >= 0) & (zz < nz))
+            def _():
+                stage(zz)
+
+        @pl.when(i < steps)
+        def _():
+            staged(i, functools.partial(column_stage, i))
+
+        @pl.when((i >= lag) & (i < steps + lag))
+        def _():
+            staged(i - lag, corner_stage)
+
+        @pl.when(i == 2 * lag)
+        def _():
+            vocab_copy.wait()
+            for k in range(1, nz):
+                zk = me.behind(k)
+                remote(
+                    target, targets.at[zk], tgt_send.at[k - 1], tgt_recv.at[k - 1], p, me.at(zk)
+                ).wait_recv()
+            for q in range(nz):
+                for j in range(group // lanes):
+                    cut = slice(j * lanes, (j + 1) * lanes)
+                    for k in range(2 * topk):
+                        columns_of[q, cut, k : k + 1] = rows_to_column(targets[q, k : k + 1, cut])
+
+        @pl.when(i >= 2 * lag)
+        def _():
+            staged(i - 2 * lag, compute_stage)
+
+        return 0
+
+    lax.fori_loop(0, steps + 2 * lag, gather_step, 0)
+    normed_copy = pltpu.make_async_copy(gathered, normed_hbm, out_sem)
+    normed_copy.start()
+
+    def plane_stat(kind):
+        return remote(stat, stat_plane.at[kind], st_send.at[kind], st_recv.at[kind], me.plane[kind], me.dp)
+
+    for kind in range(3):
+        plane_stat(kind).start()
+
+    def combined(mine, others):
+        lse = [mine[:nz]] + [o[:nz] for o in others]
+        top = functools.reduce(jnp.maximum, lse)
+        total = sum(jnp.exp(v - top) for v in lse)
+        return top + jnp.log(total), mine[nz:] + sum(o[nz:] for o in others)
+
+    for kind in range(3):
+        plane_stat(kind).wait_recv()
+    lse, tgt = combined(stat[...], [stat_plane[kind] for kind in range(3)])
+    stat_mid[0:nz] = lse
+    stat_mid[nz : 2 * nz] = tgt
+
+    def line_stat(k):
+        return remote(
+            stat_mid, stat_line.at[k - 1], st_send.at[2 + k], st_recv.at[2 + k], p, me.at(me.ahead(k))
+        )
+
+    for k in range(1, nz):
+        line_stat(k).start()
+    for k in range(1, nz):
+        line_stat(k).wait_recv()
+    lse, tgt = combined(stat_mid[...], [stat_line[k] for k in range(nz - 1)])
+    for kind in range(3):
+        plane_stat(kind).wait_send()
+    stat[0:nz] = lse
+    stat[nz : 2 * nz] = tgt
+    mine = pl.ds(pl.multiple_of(p * rows, rows), rows)
+    own_at = lax.broadcasted_iota(jnp.int32, (2 * nz, rows), 0)
+    own_lse = jnp.sum(jnp.where(own_at == z, stat[:, mine], 0.0), axis=0, keepdims=True)
+    own_tgt = jnp.sum(jnp.where(own_at == nz + z, stat[:, mine], 0.0), axis=0, keepdims=True)
+    losses_out[...] = own_lse - own_tgt + z_weight * own_lse * own_lse
+
+    def grads_copy(q):
+        return pltpu.make_async_copy(grads.at[lax.rem(q, 2)], grads_hbm.at[q], grads_sem.at[lax.rem(q, 2)])
+
+    def grads_plane(q, _):
+        @pl.when(q >= 2)
+        def _():
+            grads_copy(q - 2).wait()
+
+        for j in range(group // lanes):
+            cut = slice(j * lanes, (j + 1) * lanes)
+            lse_col[cut, :] = rows_to_column(row_of(stat, q, cut))
+
+        def some(i, _):
+            r = pl.ds(pl.multiple_of(i * chunk, chunk), chunk)
+            norm = lse_col[r, :]
+            factor = loss_scale * (1.0 + 2.0 * z_weight * norm)
+            grads[lax.rem(q, 2), r, :] = (
+                jnp.exp(scores[q, r, :] - norm) * factor - loss_scale * wanted_of(q, r)
+            ).astype(bf16)
+            return 0
+
+        lax.fori_loop(0, group // chunk, some, 0)
+        grads_copy(q).start()
+        return 0
+
+    lax.fori_loop(0, nz, grads_plane, 0)
+    for q in range(max(nz - 2, 0), nz):
+        grads_copy(q).wait()
+    normed_copy.wait()
+
+    for k in range(1, nz):
+        target_copy(k).wait_send()
+        line_stat(k).wait_send()
+    for t in range(tiles):
+        for kind in range(3):
+            piece(kind, t).wait_send()
+    for zz in range(nz):
+        to_x(zz).wait_send()
+        to_y(zz).wait_send()
+        corner_y(zz).wait_send()
+
+        @pl.when((zz <= z) & (z + 1 < nz))
+        def _():
+            up(zz).wait_send()
+
+        @pl.when((zz >= z) & (z > 0))
+        def _():
+            below(zz).wait_send()
+
+
+def backward_kernel(
+    nz,
+    normed_hbm,
+    grads_hbm,
+    vocab_hbm,
+    stream,
+    final_gain,
+    vgrad_hbm,
+    sgrad_out,
+    normed,
+    grads,
+    vocab,
+    turned,
+    block,
+    core_send_buf,
+    core_recv_buf,
+    far_send_buf,
+    far_recv_buf,
+    part,
+    first,
+    second,
+    line_recv_buf,
+    total,
+    in_sem,
+    core_send,
+    core_recv,
+    far_send,
+    far_recv,
+    hop_send,
+    hop_recv,
+    line_send,
+    line_recv,
+    out_sem,
+):
+    me = Place(nz)
+    p, z, c = me.p, me.z, me.c
+    rows, width = stream.shape
+    group = grads.shape[1]
+    tokens = nz * group
+    span = vocab.shape[1]
+    deep = width // (nz * CORES)
+
+    loads = [
+        pltpu.make_async_copy(normed_hbm, normed, in_sem.at[0]),
+        pltpu.make_async_copy(grads_hbm, grads, in_sem.at[1]),
+        pltpu.make_async_copy(
+            vocab_hbm.at[:, pl.ds(pl.multiple_of(z * span, span), span)], vocab, in_sem.at[2]
+        ),
+    ]
+    for load in loads:
+        load.start()
+
+    partner = me.dp + 1 - 2 * c
+    greet(
+        [(p, partner), (me.px, me.dp), (me.py, me.dp)] + [(p, me.at(me.ahead(k))) for k in range(1, nz)]
+    )
+    loads[0].wait()
+    loads[1].wait()
+
+    def core_copy(i):
+        return remote(
+            core_send_buf.at[lax.rem(i, 2)], core_recv_buf.at[i], core_send.at[i], core_recv.at[i], p, partner
+        )
+
+    def far_copy(k, zk):
+        return remote(
+            far_send_buf.at[k - 1], far_recv_buf.at[z], far_send.at[k - 1], far_recv.at[k - 1], p, me.at(zk)
+        )
+
+    def product(dest, store):
+        at = pl.ds(pl.multiple_of(dest * deep, deep), deep)
+        for q in range(nz):
+            turned[:, q * group : (q + 1) * group] = normed[q, :, at].T
+
+        def tile(t, _):
+            cut = pl.ds(pl.multiple_of(t * TILE, TILE), TILE)
+            store(
+                cut,
+                jnp.dot(
+                    turned[...], grads[:, :, cut].reshape(tokens, TILE), preferred_element_type=f32
+                ),
+            )
+            return 0
+
+        lax.fori_loop(0, span // TILE, tile, 0)
+
+    def vocab_step(i, _):
+        k = i + 1
+        zk = me.ahead(k)
+
+        @pl.when(i >= 2)
+        def _():
+            core_copy(i - 2).wait_send()
+
+        def to_core(cut, value):
+            core_send_buf[lax.rem(i, 2), :, cut] = value.astype(bf16)
+
+        product(zk * CORES + 1 - c, to_core)
+        core_copy(i).start()
+
+        def to_block(cut, value):
+            block[:, cut] = value
+
+        product(me.at(zk), to_block)
+        core_copy(i).wait_recv()
+
+        def add(j, _):
+            r = pl.ds(pl.multiple_of(j * 32, 32), 32)
+            value = (block[r, :] + core_recv_buf[i, r, :].astype(f32)).astype(bf16)
+
+            @pl.when(k < nz)
+            def _():
+                far_send_buf[k - 1, r, :] = value
+
+            @pl.when(k == nz)
+            def _():
+                far_recv_buf[z, r, :] = value
+
+            return 0
+
+        lax.fori_loop(0, deep // 32, add, 0)
+
+        @pl.when(k < nz)
+        def _():
+            far_copy(k, zk).start()
+
+        return 0
+
+    lax.fori_loop(0, nz, vocab_step, 0)
+    loads[2].wait()
+
+    def at_block(q):
+        return pl.ds(pl.multiple_of(q * rows, rows), rows)
+
+    def hop(zz, slot):
+        near, target = (me.px, me.px) if zz % 2 == 0 else (me.py, me.py)
+        q = near if slot == 0 else me.pd
+        return remote(
+            part.at[zz, at_block(q), :],
+            first.at[zz, slot],
+            hop_send.at[zz, slot],
+            hop_recv.at[zz, slot],
+            target,
+            me.dp,
+        )
+
+    def turn(zz):
+        target = me.py if zz % 2 == 0 else me.px
+        return remote(part.at[zz, at_block(target), :], second.at[zz], hop_send.at[zz, 2], hop_recv.at[zz, 2], target, me.dp)
+
+    def line_up(zz):
+        return remote(
+            part.at[zz, at_block(p), :], line_recv_buf.at[zz, 0], line_send.at[zz], line_recv.at[zz, 0], p, me.dp + CORES
+        )
+
+    def line_down(zz):
+        return remote(
+            part.at[zz, at_block(p), :], line_recv_buf.at[zz, 1], line_send.at[zz], line_recv.at[zz, 1], p, me.dp - CORES
+        )
+
+    step = 16
+    pieces = rows // step
+
+    def matmul_stage(zz):
+        def tile(t, _):
+            cut = pl.ds(pl.multiple_of(t * TILE, TILE), TILE)
+            part[zz, :, cut] = lax.dot_general(
+                grads[zz], vocab[cut, :], (((1,), (1,)), ((), ())), preferred_element_type=f32
+            ).astype(bf16)
+            return 0
+
+        lax.fori_loop(0, width // TILE, tile, 0)
+        hop(zz, 1).start()
+        hop(zz, 0).start()
+
+    def turn_stage(zz):
+        hop(zz, 1).wait_recv()
+        q = me.py if zz % 2 == 0 else me.px
+
+        def some(i, _):
+            r = pl.ds(pl.multiple_of(i * step, step), step)
+            at = pl.ds(pl.multiple_of(q * rows + i * step, step), step)
+            part[zz, at, :] = (part[zz, at, :].astype(f32) + first[zz, 1, r, :].astype(f32)).astype(bf16)
+            return 0
+
+        lax.fori_loop(0, pieces, some, 0)
+        turn(zz).start()
+
+    def line_stage(zz):
+        hop(zz, 0).wait_recv()
+        turn(zz).wait_recv()
+
+        @pl.when((zz >= z) & (z > 0))
+        def _():
+            line_up(zz).wait_recv()
+
+        @pl.when((zz <= z) & (z + 1 < nz))
+        def _():
+            line_down(zz).wait_recv()
+
+        def some(i, _):
+            r = pl.ds(pl.multiple_of(i * step, step), step)
+            at = pl.ds(pl.multiple_of(p * rows + i * step, step), step)
+            value = (
+                part[zz, at, :].astype(f32) + first[zz, 0, r, :].astype(f32) + second[zz, r, :].astype(f32)
+            )
+            total[r, :] = value
+
+            @pl.when((zz >= z) & (z > 0))
+            def _():
+                total[r, :] = total[r, :] + line_recv_buf[zz, 0, r, :].astype(f32)
+
+            @pl.when((zz <= z) & (z + 1 < nz))
+            def _():
+                total[r, :] = total[r, :] + line_recv_buf[zz, 1, r, :].astype(f32)
+
+            @pl.when(zz != z)
+            def _():
+                part[zz, at, :] = total[r, :].astype(bf16)
+
+            @pl.when(zz == z)
+            def _():
+                rows_of = stream[r, :]
+                inverse = lax.rsqrt(jnp.mean(rows_of * rows_of, axis=1, keepdims=True) + epsilon)
+                upstream = total[r, :] * final_gain[...]
+                sgrad_out[r, :] = inverse * (
+                    upstream
+                    - rows_of * inverse * inverse * jnp.mean(upstream * rows_of, axis=1, keepdims=True)
+                )
+
+            return 0
+
+        lax.fori_loop(0, pieces, some, 0)
+
+        @pl.when(zz > z)
+        def _():
+            line_up(zz).start()
+
+        @pl.when(zz < z)
+        def _():
+            line_down(zz).start()
+
+    order = []
+    low, high = 0, nz - 1
+    while low <= high:
+        order.append(high)
+        if low < high:
+            order.append(low)
+        low, high = low + 1, high - 1
+    for i in range(nz + 2):
+        if i < nz:
+            matmul_stage(order[i])
+        if 1 <= i <= nz:
+            turn_stage(order[i - 1])
+        if 2 <= i:
+            line_stage(order[i - 2])
+
+    def out_copy(q):
+        return pltpu.make_async_copy(
+            far_recv_buf.at[q], vgrad_hbm.at[:, pl.ds(pl.multiple_of(q * span, span), span)], out_sem.at[q]
+        )
+
+    out_copy(z).start()
+    for k in range(1, nz):
+        zk = me.behind(k)
+        remote(
+            far_send_buf.at[k - 1], far_recv_buf.at[zk], far_send.at[k - 1], far_recv.at[k - 1], p, me.at(zk)
+        ).wait_recv()
+        out_copy(zk).start()
+    for q in range(nz):
+        out_copy(q).wait()
+
+    for k in range(1, nz):
+        far_copy(k, me.ahead(k)).wait_send()
+    for i in range(max(nz - 2, 0), nz):
+        core_copy(i).wait_send()
+    for zz in range(nz):
+        hop(zz, 0).wait_send()
+        hop(zz, 1).wait_send()
+        turn(zz).wait_send()
+
+        @pl.when(zz != z)
+        def _():
+            line_up(zz).wait_send()
+
+
+def vmem():
+    return pl.BlockSpec(memory_space=pltpu.VMEM)
+
+
+def anywhere():
+    return pl.BlockSpec(memory_space=pl.ANY)
+
+
+def fast_shards(
+    nz, hidden_act, down_weight, residual, post_gain, final_gain, vocab, vocab_bias, target_ids, target_weights
+):
+    rows, width = residual.shape
+    group, hidden_units = hidden_act.shape
+    columns = vocab.shape[1]
+    span = columns // nz
+    topk = target_ids.shape[1]
+    tiles = width // TILE
+    deep = width // (nz * CORES)
+    dma = pltpu.SemaphoreType.DMA
+    target = jnp.concatenate([target_ids.astype(f32), target_weights], axis=1).T
+    normed, grads, stream, losses = pl.pallas_call(
+        functools.partial(forward_kernel, nz, topk),
+        name="forward",
+        out_shape=(
+            jax.ShapeDtypeStruct((nz, group, width), bf16),
+            jax.ShapeDtypeStruct((nz, group, span), bf16),
+            jax.ShapeDtypeStruct((rows, width), f32),
+            jax.ShapeDtypeStruct((1, rows), f32),
+        ),
+        in_specs=[vmem(), anywhere(), vmem(), vmem(), vmem(), anywhere(), vmem(), vmem()],
+        out_specs=(anywhere(), anywhere(), vmem(), vmem()),
+        scratch_shapes=[
+            pltpu.VMEM((hidden_units, width), bf16),
+            pltpu.VMEM((width, span), bf16),
+            pltpu.VMEM((group, TILE), f32),
+            pltpu.VMEM((rows, width), f32),
+            pltpu.VMEM((group, width), bf16),
+            pltpu.VMEM((3, rows, width), bf16),
+            pltpu.VMEM((nz, group, width), bf16),
+            pltpu.VMEM((nz, group, span), f32),
+            pltpu.VMEM((nz, 2 * topk, group), f32),
+            pltpu.VMEM((nz, group, 2 * topk), f32),
+            pltpu.VMEM((group, 1), f32),
+            pltpu.VMEM((group, 1), f32),
+            pltpu.VMEM((2 * nz, group), f32),
+            pltpu.VMEM((3, 2 * nz, group), f32),
+            pltpu.VMEM((2 * nz, group), f32),
+            pltpu.VMEM((nz - 1, 2 * nz, group), f32),
+            pltpu.VMEM((2, group, span), bf16),
+            dma((tiles,)),
+            dma,
+            dma((nz - 1,)),
+            dma((nz - 1,)),
+            dma((3, tiles)),
+            dma((3, tiles)),
+            dma((nz, 5)),
+            dma((nz, 4)),
+            dma((nz + 2,)),
+            dma((nz + 2,)),
+            dma,
+            dma((2,)),
+        ],
+        compiler_params=pltpu.CompilerParams(
+            collective_id=0, has_side_effects=True, vmem_limit_bytes=66 * 1000 * 1000
+        ),
+    )(
+        hidden_act,
+        down_weight,
+        residual,
+        post_gain[None, :],
+        final_gain[None, :],
+        vocab,
+        vocab_bias[None, :],
+        target,
+    )
+    vocab_grad, stream_grad = pl.pallas_call(
+        functools.partial(backward_kernel, nz),
+        name="backward",
+        out_shape=(
+            jax.ShapeDtypeStruct((deep, columns), bf16),
+            jax.ShapeDtypeStruct((rows, width), f32),
+        ),
+        in_specs=[anywhere(), anywhere(), anywhere(), vmem(), vmem()],
+        out_specs=(anywhere(), vmem()),
+        scratch_shapes=[
+            pltpu.VMEM((nz, group, width), bf16),
+            pltpu.VMEM((nz, group, span), bf16),
+            pltpu.VMEM((width, span), bf16),
+            pltpu.VMEM((deep, nz * group), bf16),
+            pltpu.VMEM((deep, span), f32),
+            pltpu.VMEM((2, deep, span), bf16),
+            pltpu.VMEM((nz, deep, span), bf16),
+            pltpu.VMEM((nz - 1, deep, span), bf16),
+            pltpu.VMEM((nz, deep, span), bf16),
+            pltpu.VMEM((nz, group, width), bf16),
+            pltpu.VMEM((nz, 2, rows, width), bf16),
+            pltpu.VMEM((nz, rows, width), bf16),
+            pltpu.VMEM((nz, 2, rows, width), bf16),
+            pltpu.VMEM((rows, width), f32),
+            dma((3,)),
+            dma((nz,)),
+            dma((nz,)),
+            dma((nz - 1,)),
+            dma((nz - 1,)),
+            dma((nz, 3)),
+            dma((nz, 3)),
+            dma((nz,)),
+            dma((nz, 2)),
+            dma((nz,)),
+        ],
+        compiler_params=pltpu.CompilerParams(
+            collective_id=1, has_side_effects=True, vmem_limit_bytes=66 * 1000 * 1000
+        ),
+    )(normed, grads, vocab, stream, final_gain[None, :])
+    return losses[0], stream_grad, vocab_grad.astype(f32)
 
 
 def inverse_rms(values):
     return lax.rsqrt(jnp.mean(values * values, axis=-1, keepdims=True) + epsilon)
 
 
-def shards(
+def general_shards(
     hidden_act,
     down_weight,
     residual,
@@ -100,4 +918,7 @@
         P("dp", None),
     )
     out_specs = (P(("dp", "vp")), P(("dp", "vp"), None), P("dp", "vp"))
-    return jax.shard_map(shards, mesh=mesh, in_specs=in_specs, out_specs=out_specs, check_vma=False)
+    body = general_shards
+    if mesh.shape["vp"] == PLANE and mesh.shape["dp"] % CORES == 0:
+        body = functools.partial(fast_shards, mesh.shape["dp"] // CORES)
+    return jax.shard_map(body, mesh=mesh, in_specs=in_specs, out_specs=out_specs, check_vma=False)

time: 640 us -> 367 us (0.57); the launches traced: 633 us -> 367 us
  waiting for transfers between devices: 455 us -> 0 us
  Pallas kernels: 0 us -> 356 us
  matrix products: 102 us -> 0 us
  other arithmetic: 50.3 us -> 8.68 us
  between operations: 14.5 us -> 0.66 us
  blocking collectives: 8.32 us -> 0 us
    reduce_scatter x6 -> x0, waiting for transfers between devices: 420 us -> none  [the longest x4 355 us: shards(): pieces.append(lax.psum_scatter(grad, 'dp', scatter_dimension=0, tiled=True))]
    pallas_call x0 -> x2, Pallas kernels: none -> 356 us  [the longest x1 207 us: fast_shards(): pl.pallas_call(functools.partial(backward_kernel, nz), name='backward', o...]
    dot_general x7 -> x0, matrix products: 102 us -> none  [the longest x4 40.4 us: shards(): lax.dot_general(gathered, part, (((0,), (0,)), ((), ())), preferred_eleme...]
    all_gather x1 -> x0, waiting for transfers between devices: 34.7 us -> none  [shards(): gathered = lax.all_gather(normed, 'vp', axis=0, tiled=True)]
    reduce_sum x5 -> x0, other arithmetic: 21.1 us -> none  [the longest x1 16.2 us: shards(): local_sum = jnp.sum(jnp.exp(scores - local_max[:, None]), axis=1)]
    convert_element_type x2, other arithmetic: 21 us -> 7.37 us  [the longest x1 6.67 us: fast_shards(): return (losses[0], stream_grad, vocab_grad.astype(f32))]
    all_gather x1 -> x0, blocking collectives: 8.32 us -> none  [shards(): lax.all_gather(jnp.stack([local_max, local_sum, local_target]), 'vp', axi...]
  transfers between devices with their start and end apart: 7 -> 0, of which waited for: 7 -> 0; matrix products, arithmetic and copies ran while one was open for 7% -> 0% of each run, Pallas kernels for 0% -> 0%
where the time goes in v1:
time: 367 us
  Pallas kernels  356 us (97%)
  other arithmetic  8.68 us (2%)
    pallas_call x1, Pallas kernels, fast_shards(): pl.pallas_call(functools.partial(backward_kernel, nz), name='backward', o...  207 us
    pallas_call x1, Pallas kernels, fast_shards(): pl.pallas_call(functools.partial(forward_kernel, nz, topk), name='forward...  149 us

profile of v1, /device:TPU:8, one launch (start us, length us, event | category | flops | bytes accessed | tf_op | source)
XLA Modules:
  0.0 366.9 jit_solution(2197482235510466818)
XLA Ops:
  0.6 0.7 convert_element_type.6
  1.3 1.3 maximum_bitcast_fusion.target
  2.6 148.6 %forward.1 = (bf16[4,512,2048]{2,1,0:T(8,128)(2,1)}, bf16[4,512,2048]{2,1,0:T(8,128)(2,1)}, f32[128,2048]{1,0:T(8,128)}, f32[1,128]{1,0:T(1,128)}) custom-call(bf16[512,2048]{1,0:T(8,128)(2,1)} %hidden.1, bf16[2048,2048]{1,0:T(8,128)(2,1)} %down_hbm.1, bf16[128,2048]{1,0:T(8,128)(2,1)} %resid.1, f32[1,2048]{1,0:T(1,128)} %bitcast.9, f32[1,2048]{1,0:T(1,128)} %bitcast.7, ...), custom_call_target="tpu_custom_call" | custom-call | tf_op jit(solution)/shard_map/forward/pallas_call | solution.py:735
  151.2 207.5 %backward.1 = (bf16[256,8192]{1,0:T(8,128)(2,1)}, f32[128,2048]{1,0:T(8,128)}) custom-call(bf16[4,512,2048]{2,1,0:T(8,128)(2,1)} %get-tuple-element.10.normed_hbm, bf16[4,512,2048]{2,1,0:T(8,128)(2,1)} %get-tuple-element.11.grads_hbm, bf16[2048,8192]{1,0:T(8,128)(2,1)} %vocab_hbm.3, f32[128,2048]{1,0:T(8,128)} %get-tuple-element.12.stream, f32[1,2048]{1,0:T(1,128)} %bitcast.8), custom_call_target="tpu_custom_call" | custom-call | tf_op jit(solution)/shard_map/backward/pallas_call | solution.py:790
  358.7 0.0 copy-start.1
  358.7 0.0 copy-start
  358.7 6.7 %convert_element_type.7 = f32[256,8192]{1,0:T(8,128)} convert(bf16[256,8192]{1,0:T(8,128)(2,1)} %get-tuple-element.14) | non-fusion elementwise | flops 2097152 | bytes 12582912 | tf_op jit(solution)/shard_map/convert_element_type | solution.py:829
  365.4 0.0 copy-done.1
  365.4 0.5 copy.14
  365.9 0.0 copy-done
  365.9 1.0 copy.15
Async XLA Ops:
  358.7 6.7 %copy-start.1 = (f32[1,128]{1,0:T(1,128)S(1)}, f32[1,128]{1,0:T(1,128)}, u32[]{:S(2)}) copy-start(f32[1,128]{1,0:T(1,128)} %get-tuple-element.9) | copy-start | bytes 1540
  358.7 7.2 %copy-start = (f32[128,2048]{1,0:T(8,128)S(1)}, f32[128,2048]{1,0:T(8,128)}, u32[]{:S(2)}) copy-start(f32[128,2048]{1,0:T(8,128)} %get-tuple-element.19) | copy-start | bytes 3145732

commit v2 on v1

--- a/solution.py
+++ b/solution.py
@@ -10,6 +10,7 @@
 MESH = pl.DeviceIdType.MESH
 CORES = 2
 PLANE = 4
+LINE = 4
 TILE = 512
 CHUNKS = 4
 
@@ -252,12 +253,10 @@
     lanes = 128
 
     def wanted_of(zz, r):
-        total = None
+        total = 0.0
         for k in range(topk):
             ids = columns_of[zz, r, k : k + 1] - first_column.astype(f32)
-            weight = columns_of[zz, r, topk + k : topk + k + 1]
-            term = jnp.where(ids == position, weight, 0.0)
-            total = term if total is None else total + term
+            total = jnp.where(ids == position, columns_of[zz, r, topk + k : topk + k + 1], total)
         return total
 
     row_at = lax.broadcasted_iota(jnp.int32, (2 * nz, lanes), 0)
@@ -266,33 +265,43 @@
     def row_of(ref, q, cut):
         return jnp.sum(jnp.where(row_at == q, ref[:, cut], 0.0), axis=0, keepdims=True)
 
-    def compute_stage(zz):
-        landed(zz, 3, me.pd).wait_recv()
+    pair = 2 * rows
+
+    def compute_pair(zz, which):
+        base = which * pair
 
         def tile(t, _):
             cut = pl.ds(pl.multiple_of(t * TILE, TILE), TILE)
             at = pl.ds(pl.multiple_of(z * span + t * TILE, TILE), TILE)
-            scores[zz, :, cut] = (
-                jnp.dot(gathered[zz], vocab[:, cut], preferred_element_type=f32) + bias[:, at]
+            r = pl.ds(pl.multiple_of(base, pair), pair)
+            scores[zz, r, cut] = (
+                jnp.dot(gathered[zz, r, :], vocab[:, cut], preferred_element_type=f32) + bias[:, at]
             )
             return 0
 
         lax.fori_loop(0, span // TILE, tile, 0)
 
         def stats(i, _):
-            r = pl.ds(pl.multiple_of(i * chunk, chunk), chunk)
+            r = pl.ds(pl.multiple_of(base + i * chunk, chunk), chunk)
+            at = pl.ds(pl.multiple_of(i * chunk, chunk), chunk)
             values = scores[zz, r, :]
             largest = jnp.max(values, axis=1, keepdims=True)
             total = jnp.sum(jnp.exp(values - largest), axis=1, keepdims=True)
-            lse_col[r, :] = largest + jnp.log(total)
-            tgt_col[r, :] = jnp.sum(wanted_of(zz, r) * values, axis=1, keepdims=True)
+            lse_col[at, :] = largest + jnp.log(total)
+            tgt_col[at, :] = jnp.sum(wanted_of(zz, r) * values, axis=1, keepdims=True)
             return 0
 
-        lax.fori_loop(0, group // chunk, stats, 0)
-        for j in range(group // lanes):
+        lax.fori_loop(0, pair // chunk, stats, 0)
+        for j in range(pair // lanes):
             cut = slice(j * lanes, (j + 1) * lanes)
-            kept = jnp.where(row_at == zz, column_to_row(lse_col[cut, :]), stat[:, cut])
-            stat[:, cut] = jnp.where(row_at == nz + zz, column_to_row(tgt_col[cut, :]), kept)
+            at = pl.ds(pl.multiple_of(base + j * lanes, lanes), lanes)
+            kept = jnp.where(row_at == zz, column_to_row(lse_col[cut, :]), stat[:, at])
+            stat[:, at] = jnp.where(row_at == nz + zz, column_to_row(tgt_col[cut, :]), kept)
+
+    def compute_stage(zz):
+        compute_pair(zz, p // 2)
+        landed(zz, 3, me.pd).wait_recv()
+        compute_pair(zz, 1 - p // 2)
 
     steps = 2 * nz - 1
     lag = 2
@@ -325,8 +334,12 @@
             for q in range(nz):
                 for j in range(group // lanes):
                     cut = slice(j * lanes, (j + 1) * lanes)
-                    for k in range(2 * topk):
-                        columns_of[q, cut, k : k + 1] = rows_to_column(targets[q, k : k + 1, cut])
+                    ids = [targets[q, k : k + 1, cut] for k in range(topk)]
+                    weights = [targets[q, topk + k : topk + k + 1, cut] for k in range(topk)]
+                    for k in range(topk):
+                        whole = sum(jnp.where(ids[j] == ids[k], weights[j], 0.0) for j in range(topk))
+                        columns_of[q, cut, k : k + 1] = rows_to_column(ids[k])
+                        columns_of[q, cut, topk + k : topk + k + 1] = rows_to_column(whole)
 
         @pl.when(i >= 2 * lag)
         def _():
@@ -448,7 +461,6 @@
     first,
     second,
     line_recv_buf,
-    total,
     in_sem,
     core_send,
     core_recv,
@@ -468,26 +480,34 @@
     span = vocab.shape[1]
     deep = width // (nz * CORES)
 
-    loads = [
-        pltpu.make_async_copy(normed_hbm, normed, in_sem.at[0]),
-        pltpu.make_async_copy(grads_hbm, grads, in_sem.at[1]),
-        pltpu.make_async_copy(
-            vocab_hbm.at[:, pl.ds(pl.multiple_of(z * span, span), span)], vocab, in_sem.at[2]
-        ),
-    ]
-    for load in loads:
-        load.start()
+    ahead = sorted(range(1, nz), key=lambda k: abs(2 * k - nz)) + [nz]
+
+    def normed_load(i, mine):
+        side = me.c if mine else 1 - me.c
+        at = pl.ds(pl.multiple_of((me.ahead(ahead[i]) * CORES + side) * deep, deep), deep)
+        return pltpu.make_async_copy(normed_hbm.at[:, :, at], normed.at[:, :, at], in_sem.at[2 + 2 * i + mine])
+
+    grads_load = pltpu.make_async_copy(grads_hbm, grads, in_sem.at[0])
+    vocab_load = pltpu.make_async_copy(
+        vocab_hbm.at[:, pl.ds(pl.multiple_of(z * span, span), span)], vocab, in_sem.at[1]
+    )
+    grads_load.start()
+    normed_load(0, 0).start()
+    normed_load(0, 1).start()
+    vocab_load.start()
+    for i in range(1, nz):
+        normed_load(i, 0).start()
+        normed_load(i, 1).start()
 
     partner = me.dp + 1 - 2 * c
     greet(
         [(p, partner), (me.px, me.dp), (me.py, me.dp)] + [(p, me.at(me.ahead(k))) for k in range(1, nz)]
     )
-    loads[0].wait()
-    loads[1].wait()
+    grads_load.wait()
 
     def core_copy(i):
         return remote(
-            core_send_buf.at[lax.rem(i, 2)], core_recv_buf.at[i], core_send.at[i], core_recv.at[i], p, partner
+            core_send_buf.at[i % 2], core_recv_buf.at[i], core_send.at[i], core_recv.at[i], p, partner
         )
 
     def far_copy(k, zk):
@@ -512,22 +532,24 @@
 
         lax.fori_loop(0, span // TILE, tile, 0)
 
-    def vocab_step(i, _):
-        k = i + 1
+    def vocab_step(i):
+        k = ahead[i]
         zk = me.ahead(k)
-
-        @pl.when(i >= 2)
-        def _():
+        if i >= 2:
             core_copy(i - 2).wait_send()
 
         def to_core(cut, value):
-            core_send_buf[lax.rem(i, 2), :, cut] = value.astype(bf16)
+            core_send_buf[i % 2, :, cut] = value.astype(bf16)
+
+        normed_load(i, 0).wait()
 
         product(zk * CORES + 1 - c, to_core)
         core_copy(i).start()
 
         def to_block(cut, value):
             block[:, cut] = value
+
+        normed_load(i, 1).wait()
 
         product(me.at(zk), to_block)
         core_copy(i).wait_recv()
@@ -536,32 +558,22 @@
             r = pl.ds(pl.multiple_of(j * 32, 32), 32)
             value = (block[r, :] + core_recv_buf[i, r, :].astype(f32)).astype(bf16)
 
-            @pl.when(k < nz)
-            def _():
+            if k < nz:
                 far_send_buf[k - 1, r, :] = value
-
-            @pl.when(k == nz)
-            def _():
+            else:
                 far_recv_buf[z, r, :] = value
-
             return 0
 
         lax.fori_loop(0, deep // 32, add, 0)
-
-        @pl.when(k < nz)
-        def _():
+        if k < nz:
             far_copy(k, zk).start()
-
-        return 0
-
-    lax.fori_loop(0, nz, vocab_step, 0)
-    loads[2].wait()
 
     def at_block(q):
         return pl.ds(pl.multiple_of(q * rows, rows), rows)
 
     def hop(zz, slot):
-        near, target = (me.px, me.px) if zz % 2 == 0 else (me.py, me.py)
+        even = not isinstance(zz, int) or zz % 2 == 0
+        near, target = (me.px, me.px) if even else (me.py, me.py)
         q = near if slot == 0 else me.pd
         return remote(
             part.at[zz, at_block(q), :],
@@ -573,17 +585,36 @@
         )
 
     def turn(zz):
-        target = me.py if zz % 2 == 0 else me.px
+        even = not isinstance(zz, int) or zz % 2 == 0
+        target = me.py if even else me.px
         return remote(part.at[zz, at_block(target), :], second.at[zz], hop_send.at[zz, 2], hop_recv.at[zz, 2], target, me.dp)
 
-    def line_up(zz):
+    half = z // 2
+    inner = z * (LINE - 1 - z) // 2
+    beside = z + 1 - 2 * lax.rem(z, 2)
+
+    def far_plane(j):
+        return (1 - half) * (LINE - 1) + (2 * half - 1) * j
+
+    def line_far(zz):
+        target = beside + inner * (zz - beside)
         return remote(
-            part.at[zz, at_block(p), :], line_recv_buf.at[zz, 0], line_send.at[zz], line_recv.at[zz, 0], p, me.dp + CORES
+            part.at[zz, at_block(p), :],
+            line_recv_buf.at[zz, 0],
+            line_send.at[zz],
+            line_recv.at[zz, 0],
+            p,
+            me.at(target),
         )
 
-    def line_down(zz):
+    def line_near(zz):
         return remote(
-            part.at[zz, at_block(p), :], line_recv_buf.at[zz, 1], line_send.at[zz], line_recv.at[zz, 1], p, me.dp - CORES
+            part.at[zz, at_block(p), :],
+            line_recv_buf.at[zz, 1],
+            line_send.at[zz],
+            line_recv.at[zz, 1],
+            p,
+            me.at(beside),
         )
 
     step = 16
@@ -614,59 +645,67 @@
         lax.fori_loop(0, pieces, some, 0)
         turn(zz).start()
 
-    def line_stage(zz):
-        hop(zz, 0).wait_recv()
-        turn(zz).wait_recv()
-
-        @pl.when((zz >= z) & (z > 0))
-        def _():
-            line_up(zz).wait_recv()
-
-        @pl.when((zz <= z) & (z + 1 < nz))
-        def _():
-            line_down(zz).wait_recv()
-
+    def plane_sum(zz, i):
+        r = pl.ds(pl.multiple_of(i * step, step), step)
+        at = pl.ds(pl.multiple_of(p * rows + i * step, step), step)
+        return (
+            part[zz, at, :].astype(f32) + first[zz, 0, r, :].astype(f32) + second[zz, r, :].astype(f32)
+        )
+
+    def store_sum(zz, added):
         def some(i, _):
             r = pl.ds(pl.multiple_of(i * step, step), step)
             at = pl.ds(pl.multiple_of(p * rows + i * step, step), step)
-            value = (
-                part[zz, at, :].astype(f32) + first[zz, 0, r, :].astype(f32) + second[zz, r, :].astype(f32)
+            value = plane_sum(zz, i)
+            if added:
+                value = value + line_recv_buf[zz, 0, r, :].astype(f32)
+            part[zz, at, :] = value.astype(bf16)
+            return 0
+
+        lax.fori_loop(0, pieces, some, 0)
+
+    def far_stage(j):
+        zz = far_plane(j)
+        hop(zz, 0).wait_recv()
+        turn(zz).wait_recv()
+
+        @pl.when(inner == 0)
+        def _():
+            store_sum(zz, False)
+
+        @pl.when(inner == 1)
+        def _():
+            line_far(zz).wait_recv()
+            store_sum(zz, True)
+
+        line_far(zz).start()
+
+    def near_stage():
+        hop(beside, 0).wait_recv()
+        turn(beside).wait_recv()
+        store_sum(beside, False)
+        line_near(beside).start()
+
+    def last_stage():
+        hop(z, 0).wait_recv()
+        turn(z).wait_recv()
+        line_far(z).wait_recv()
+        line_near(z).wait_recv()
+
+        def some(i, _):
+            r = pl.ds(pl.multiple_of(i * step, step), step)
+            value = plane_sum(z, i)
+            for k in range(2):
+                value = value + line_recv_buf[z, k, r, :].astype(f32)
+            rows_of = stream[r, :]
+            inverse = lax.rsqrt(jnp.mean(rows_of * rows_of, axis=1, keepdims=True) + epsilon)
+            upstream = value * final_gain[...]
+            sgrad_out[r, :] = inverse * (
+                upstream - rows_of * inverse * inverse * jnp.mean(upstream * rows_of, axis=1, keepdims=True)
             )
-            total[r, :] = value
-
-            @pl.when((zz >= z) & (z > 0))
-            def _():
-                total[r, :] = total[r, :] + line_recv_buf[zz, 0, r, :].astype(f32)
-
-            @pl.when((zz <= z) & (z + 1 < nz))
-            def _():
-                total[r, :] = total[r, :] + line_recv_buf[zz, 1, r, :].astype(f32)
-
-            @pl.when(zz != z)
-            def _():
-                part[zz, at, :] = total[r, :].astype(bf16)
-
-            @pl.when(zz == z)
-            def _():
-                rows_of = stream[r, :]
-                inverse = lax.rsqrt(jnp.mean(rows_of * rows_of, axis=1, keepdims=True) + epsilon)
-                upstream = total[r, :] * final_gain[...]
-                sgrad_out[r, :] = inverse * (
-                    upstream
-                    - rows_of * inverse * inverse * jnp.mean(upstream * rows_of, axis=1, keepdims=True)
-                )
-
             return 0
 
         lax.fori_loop(0, pieces, some, 0)
-
-        @pl.when(zz > z)
-        def _():
-            line_up(zz).start()
-
-        @pl.when(zz < z)
-        def _():
-            line_down(zz).start()
 
     order = []
     low, high = 0, nz - 1
@@ -675,13 +714,18 @@
         if low < high:
             order.append(low)
         low, high = low + 1, high - 1
-    for i in range(nz + 2):
-        if i < nz:
-            matmul_stage(order[i])
-        if 1 <= i <= nz:
+    for i in range(nz):
+        vocab_step(i)
+        if i == 0:
+            vocab_load.wait()
+        matmul_stage(order[i])
+        if i > 0:
             turn_stage(order[i - 1])
-        if 2 <= i:
-            line_stage(order[i - 2])
+    turn_stage(order[nz - 1])
+    far_stage(0)
+    far_stage(1)
+    near_stage()
+    last_stage()
 
     def out_copy(q):
         return pltpu.make_async_copy(
@@ -709,7 +753,7 @@
 
         @pl.when(zz != z)
         def _():
-            line_up(zz).wait_send()
+            line_near(zz).wait_send()
 
 
 def vmem():
@@ -810,8 +854,7 @@
             pltpu.VMEM((nz, 2, rows, width), bf16),
             pltpu.VMEM((nz, rows, width), bf16),
             pltpu.VMEM((nz, 2, rows, width), bf16),
-            pltpu.VMEM((rows, width), f32),
-            dma((3,)),
+            dma((2 + 2 * nz,)),
             dma((nz,)),
             dma((nz,)),
             dma((nz - 1,)),
@@ -919,6 +962,6 @@
     )
     out_specs = (P(("dp", "vp")), P(("dp", "vp"), None), P("dp", "vp"))
     body = general_shards
-    if mesh.shape["vp"] == PLANE and mesh.shape["dp"] % CORES == 0:
-        body = functools.partial(fast_shards, mesh.shape["dp"] // CORES)
+    if mesh.shape["vp"] == PLANE and mesh.shape["dp"] == LINE * CORES:
+        body = functools.partial(fast_shards, LINE)
     return jax.shard_map(body, mesh=mesh, in_specs=in_specs, out_specs=out_specs, check_vma=False)

time: 367 us -> 290 us (0.79)
  Pallas kernels: 356 us -> 277 us
    pallas_call x1, Pallas kernels: 207 us -> 128 us  [fast_shards(): pl.pallas_call(functools.partial(backward_kernel, nz), name='backward', o...]
where the time goes in v2:
time: 290 us; the launch traced here: 287 us
  Pallas kernels  277 us (96%)
  other arithmetic  8.68 us (3%)
    pallas_call x1, Pallas kernels, fast_shards(): pl.pallas_call(functools.partial(forward_kernel, nz, topk), name='forward...  148 us
    pallas_call x1, Pallas kernels, fast_shards(): pl.pallas_call(functools.partial(backward_kernel, nz), name='backward', o...  128 us
    convert_element_type x1, other arithmetic, fast_shards(): return (losses[0], stream_grad, vocab_grad.astype(f32))  6.67 us

profile of v2, /device:TPU:8, one launch (start us, length us, event | category | flops | bytes accessed | tf_op | source)
XLA Modules:
  0.0 287.4 jit_solution(15198443282295730349)
XLA Ops:
  0.6 0.7 convert_element_type.6
  1.3 1.3 maximum_bitcast_fusion.target
  2.6 148.4 %forward.1 = (bf16[4,512,2048]{2,1,0:T(8,128)(2,1)}, bf16[4,512,2048]{2,1,0:T(8,128)(2,1)}, f32[128,2048]{1,0:T(8,128)}, f32[1,128]{1,0:T(1,128)}) custom-call(bf16[512,2048]{1,0:T(8,128)(2,1)} %hidden.1, bf16[2048,2048]{1,0:T(8,128)(2,1)} %down_hbm.1, bf16[128,2048]{1,0:T(8,128)(2,1)} %resid.1, f32[1,2048]{1,0:T(1,128)} %bitcast.9, f32[1,2048]{1,0:T(1,128)} %bitcast.7, ...), custom_call_target="tpu_custom_call" | custom-call | tf_op jit(solution)/shard_map/forward/pallas_call | solution.py:779
  151.1 128.2 %backward.1 = (bf16[256,8192]{1,0:T(8,128)(2,1)}, f32[128,2048]{1,0:T(8,128)}) custom-call(bf16[4,512,2048]{2,1,0:T(8,128)(2,1)} %get-tuple-element.10.normed_hbm, bf16[4,512,2048]{2,1,0:T(8,128)(2,1)} %get-tuple-element.11.grads_hbm, bf16[2048,8192]{1,0:T(8,128)(2,1)} %vocab_hbm.3, f32[128,2048]{1,0:T(8,128)} %get-tuple-element.12.stream, f32[1,2048]{1,0:T(1,128)} %bitcast.8), custom_call_target="tpu_custom_call" | custom-call | tf_op jit(solution)/shard_map/backward/pallas_call | solution.py:834
  279.2 0.0 copy-start.1
  279.3 0.0 copy-start
  279.3 6.7 %convert_element_type.7 = f32[256,8192]{1,0:T(8,128)} convert(bf16[256,8192]{1,0:T(8,128)(2,1)} %get-tuple-element.14) | non-fusion elementwise | flops 2097152 | bytes 12582912 | tf_op jit(solution)/shard_map/convert_element_type | solution.py:872
  285.9 0.0 copy-done.1
  285.9 0.5 copy.14
  286.4 0.0 copy-done
  286.5 1.0 copy.15
Async XLA Ops:
  279.2 6.7 %copy-start.1 = (f32[1,128]{1,0:T(1,128)S(1)}, f32[1,128]{1,0:T(1,128)}, u32[]{:S(2)}) copy-start(f32[1,128]{1,0:T(1,128)} %get-tuple-element.9) | copy-start | bytes 1540
  279.3 7.2 %copy-start = (f32[128,2048]{1,0:T(8,128)S(1)}, f32[128,2048]{1,0:T(8,128)}, u32[]{:S(2)}) copy-start(f32[128,2048]{1,0:T(8,128)} %get-tuple-element.19) | copy-start | bytes 3145732

commit v3 on v2

--- a/solution.py
+++ b/solution.py
@@ -11,7 +11,7 @@
 CORES = 2
 PLANE = 4
 LINE = 4
-TILE = 512
+TILE = 1024
 CHUNKS = 4
 
 epsilon = 1e-06
@@ -124,6 +124,7 @@
     group = hidden.shape[0]
     span = vocab.shape[1]
     tiles = width // TILE
+    lanes = 128
 
     def down_copy(t):
         cut = pl.ds(pl.multiple_of(t * TILE, TILE), TILE)
@@ -169,11 +170,27 @@
         return 0
 
     lax.fori_loop(0, tiles, down_tile, 0)
+
+    for k in range(1, nz):
+        zk = me.behind(k)
+        remote(
+            target, targets.at[zk], tgt_send.at[k - 1], tgt_recv.at[k - 1], p, me.at(zk)
+        ).wait_recv()
+    for q in range(nz):
+        for j in range(group // lanes):
+            cut = slice(j * lanes, (j + 1) * lanes)
+            ids = [targets[q, k : k + 1, cut] for k in range(topk)]
+            weights = [targets[q, topk + k : topk + k + 1, cut] for k in range(topk)]
+            for k in range(topk):
+                whole = sum(jnp.where(ids[j] == ids[k], weights[j], 0.0) for j in range(topk))
+                columns_of[q, cut, k : k + 1] = rows_to_column(ids[k])
+                columns_of[q, cut, topk + k : topk + k + 1] = rows_to_column(whole)
+
     for t in range(tiles):
         for kind in range(3):
             piece(kind, t).wait_recv()
 
-    step = 16
+    step = 64
 
     def norm_rows(i, _):
         r = pl.ds(pl.multiple_of(i * step, step), step)
@@ -249,8 +266,7 @@
 
     first_column = p * vocab_hbm.shape[1] + z * span
     position = lax.broadcasted_iota(jnp.int32, (1, span), 1).astype(f32)
-    chunk = 32
-    lanes = 128
+    chunk = 128
 
     def wanted_of(zz, r):
         total = 0.0
@@ -326,20 +342,6 @@
         @pl.when(i == 2 * lag)
         def _():
             vocab_copy.wait()
-            for k in range(1, nz):
-                zk = me.behind(k)
-                remote(
-                    target, targets.at[zk], tgt_send.at[k - 1], tgt_recv.at[k - 1], p, me.at(zk)
-                ).wait_recv()
-            for q in range(nz):
-                for j in range(group // lanes):
-                    cut = slice(j * lanes, (j + 1) * lanes)
-                    ids = [targets[q, k : k + 1, cut] for k in range(topk)]
-                    weights = [targets[q, topk + k : topk + k + 1, cut] for k in range(topk)]
-                    for k in range(topk):
-                        whole = sum(jnp.where(ids[j] == ids[k], weights[j], 0.0) for j in range(topk))
-                        columns_of[q, cut, k : k + 1] = rows_to_column(ids[k])
-                        columns_of[q, cut, topk + k : topk + k + 1] = rows_to_column(whole)
 
         @pl.when(i >= 2 * lag)
         def _():
@@ -555,7 +557,7 @@
         core_copy(i).wait_recv()
 
         def add(j, _):
-            r = pl.ds(pl.multiple_of(j * 32, 32), 32)
+            r = pl.ds(pl.multiple_of(j * 128, 128), 128)
             value = (block[r, :] + core_recv_buf[i, r, :].astype(f32)).astype(bf16)
 
             if k < nz:
@@ -564,7 +566,7 @@
                 far_recv_buf[z, r, :] = value
             return 0
 
-        lax.fori_loop(0, deep // 32, add, 0)
+        lax.fori_loop(0, deep // 128, add, 0)
         if k < nz:
             far_copy(k, zk).start()
 
@@ -617,7 +619,7 @@
             me.at(beside),
         )
 
-    step = 16
+    step = 64
     pieces = rows // step
 
     def matmul_stage(zz):
@@ -774,6 +776,18 @@
     topk = target_ids.shape[1]
     tiles = width // TILE
     deep = width // (nz * CORES)
+    if width % TILE or span % TILE or deep % 128 or rows % 128 or group != PLANE * rows:
+        return general_shards(
+            hidden_act,
+            down_weight,
+            residual,
+            post_gain,
+            final_gain,
+            vocab,
+            vocab_bias,
+            target_ids,
+            target_weights,
+        )
     dma = pltpu.SemaphoreType.DMA
     target = jnp.concatenate([target_ids.astype(f32), target_weights], axis=1).T
     normed, grads, stream, losses = pl.pallas_call(

time: 290 us -> 279 us (0.962)
  Pallas kernels: 277 us -> 265 us
    pallas_call x1, Pallas kernels: 148 us -> 137 us  [fast_shards(): pl.pallas_call(functools.partial(forward_kernel, nz, topk), name='forward...]
where the time goes in v3:
time: 279 us; the launch traced here: 276 us
  Pallas kernels  265 us (95%)
  other arithmetic  8.68 us (3%)
    pallas_call x1, Pallas kernels, fast_shards(): pl.pallas_call(functools.partial(forward_kernel, nz, topk), name='forward...  137 us
    pallas_call x1, Pallas kernels, fast_shards(): pl.pallas_call(functools.partial(backward_kernel, nz), name='backward', o...  128 us
    convert_element_type x1, other arithmetic, fast_shards(): return (losses[0], stream_grad, vocab_grad.astype(f32))  6.67 us

profile of v3, /device:TPU:8, one launch (start us, length us, event | category | flops | bytes accessed | tf_op | source)
XLA Modules:
  0.0 275.8 jit_solution(16713088186747045126)
XLA Ops:
  0.6 0.7 convert_element_type.6
  1.3 1.3 maximum_bitcast_fusion.target
  2.6 137.4 %forward.1 = (bf16[4,512,2048]{2,1,0:T(8,128)(2,1)}, bf16[4,512,2048]{2,1,0:T(8,128)(2,1)}, f32[128,2048]{1,0:T(8,128)}, f32[1,128]{1,0:T(1,128)}) custom-call(bf16[512,2048]{1,0:T(8,128)(2,1)} %hidden.1, bf16[2048,2048]{1,0:T(8,128)(2,1)} %down_hbm.1, bf16[128,2048]{1,0:T(8,128)(2,1)} %resid.1, f32[1,2048]{1,0:T(1,128)} %bitcast.9, f32[1,2048]{1,0:T(1,128)} %bitcast.7, ...), custom_call_target="tpu_custom_call" | custom-call | tf_op jit(solution)/shard_map/forward/pallas_call | solution.py:793
  140.1 127.6 %backward.1 = (bf16[256,8192]{1,0:T(8,128)(2,1)}, f32[128,2048]{1,0:T(8,128)}) custom-call(bf16[4,512,2048]{2,1,0:T(8,128)(2,1)} %get-tuple-element.10.normed_hbm, bf16[4,512,2048]{2,1,0:T(8,128)(2,1)} %get-tuple-element.11.grads_hbm, bf16[2048,8192]{1,0:T(8,128)(2,1)} %vocab_hbm.3, f32[128,2048]{1,0:T(8,128)} %get-tuple-element.12.stream, f32[1,2048]{1,0:T(1,128)} %bitcast.8), custom_call_target="tpu_custom_call" | custom-call | tf_op jit(solution)/shard_map/backward/pallas_call | solution.py:848
  267.6 0.0 copy-start.1
  267.6 0.0 copy-start
  267.7 6.7 %convert_element_type.7 = f32[256,8192]{1,0:T(8,128)} convert(bf16[256,8192]{1,0:T(8,128)(2,1)} %get-tuple-element.14) | non-fusion elementwise | flops 2097152 | bytes 12582912 | tf_op jit(solution)/shard_map/convert_element_type | solution.py:886
  274.3 0.0 copy-done.1
  274.3 0.5 copy.14
  274.8 0.0 copy-done
  274.8 1.0 copy.15
Async XLA Ops:
  267.6 6.7 %copy-start.1 = (f32[1,128]{1,0:T(1,128)S(1)}, f32[1,128]{1,0:T(1,128)}, u32[]{:S(2)}) copy-start(f32[1,128]{1,0:T(1,128)} %get-tuple-element.9) | copy-start | bytes 1540
  267.6 7.2 %copy-start = (f32[128,2048]{1,0:T(8,128)S(1)}, f32[128,2048]{1,0:T(8,128)}, u32[]{:S(2)}) copy-start(f32[128,2048]{1,0:T(8,128)} %get-tuple-element.19) | copy-start | bytes 3145732
